TPU v7x, 32 devices: a whole 2x2x4 slice. The times are simulated.
32 devices in a mesh: sp: 8 (over z, y), tp: 4 (over x, core).
Axes of the slice: x: 2, y: 2, z: 4, core: 2. Of those that a mesh axis runs over, the one named last changes fastest.
Arguments:
- prompt_input: bfloat16 [2304, 2048], P('sp'), may hold values from -6 to 6
- next_input: bfloat16 [2048], replicated, may hold values from -6 to 6
- norm_gain: float32 [2048], replicated, may hold values from 0.1 to 1.9
- w_key: bfloat16 [2048, 1024], P(None, 'tp'), may hold values from -0.125 to 0.125
- w_value: bfloat16 [2048, 1024], P(None, 'tp'), may hold values from -0.125 to 0.125
- w_query: bfloat16 [2048, 1024], P(None, 'tp'), may hold values from -0.125 to 0.125
- key_offset: float32 [2304, 8], P('sp', 'tp'), may hold values from -10 to 0, as said below
Outputs:
- key_cache: bfloat16 [8, 8, 36, 1024], P('sp', None, None, 'tp')
- value_cache: bfloat16 [8, 8, 36, 1024], P('sp', None, None, 'tp')
- reading: bfloat16 [1024], replicated
Inputs may be any that keep to these rules, and one draw needn't show every extreme that they name: `key_offset`: finite log-odds offsets, one per key and head.
All inputs are finite; a program needn't handle non-finite values.
Results may differ from a plain program's by a relative error of at most 0.011.
Values may be sent and summed in bfloat16 or wider, within the bound.
A program may use at most 64 MiB of HBM per device.

v0:
```python
import jax
import jax.numpy as jnp
from jax import lax
from jax.sharding import PartitionSpec as P

HEAD_DIM = 128


def norm_rows(row_block, gain_vec):
    wide_rows = row_block.astype(jnp.float32)
    inv_rms = lax.rsqrt(jnp.mean(wide_rows * wide_rows, axis=-1, keepdims=True) + 1e-06)
    return (wide_rows * inv_rms * gain_vec).astype(jnp.bfloat16)


def shards(prompt_input, next_input, norm_gain, w_key, w_value, w_query, key_offset):
    span_len = prompt_input.shape[0]
    head_width = w_key.shape[1]
    heads_here = head_width // HEAD_DIM
    score_scale = HEAD_DIM ** (-0.5)
    slots = lax.axis_size("sp")
    sub_len = span_len // slots
    normed = norm_rows(prompt_input, norm_gain)
    key_rows = jnp.dot(normed, w_key, preferred_element_type=jnp.float32).astype(jnp.bfloat16)
    value_rows = jnp.dot(normed, w_value, preferred_element_type=jnp.float32).astype(jnp.bfloat16)
    outgoing = jnp.stack([key_rows, value_rows]).reshape(2, slots, 1, sub_len, head_width)
    arrived = lax.all_to_all(outgoing, "sp", split_axis=1, concat_axis=2, tiled=True)
    key_cache = arrived[0]
    value_cache = arrived[1]
    new_query = jnp.dot(
        norm_rows(next_input[None, :], norm_gain), w_query, preferred_element_type=jnp.float32
    )
    new_query = new_query.astype(jnp.bfloat16).reshape(heads_here, HEAD_DIM)
    key_heads = key_rows.reshape(span_len, heads_here, HEAD_DIM)
    value_heads = value_rows.reshape(span_len, heads_here, HEAD_DIM)
    logits = (
        jnp.einsum("hd,shd->sh", new_query, key_heads, preferred_element_type=jnp.float32)
        * score_scale
        + key_offset
    )
    log_breaks = jax.nn.log_sigmoid(-logits)
    inner_sum = lax.cumsum(log_breaks, axis=0, reverse=True) - log_breaks
    block_totals = jnp.sum(log_breaks, axis=0)
    every_total = lax.all_gather(block_totals[None], "sp", axis=0, tiled=True)
    block_ids = lax.broadcasted_iota(jnp.int32, every_total.shape, 0)
    carried = jnp.sum(jnp.where(block_ids > lax.axis_index("sp"), every_total, 0.0), axis=0)
    weights = jnp.exp(jax.nn.log_sigmoid(logits) + inner_sum + carried[None, :])
    partial_value = jnp.einsum("sh,shd->hd", weights, value_heads.astype(jnp.float32))
    summed = lax.psum(partial_value, "sp")
    own_read = summed.reshape(head_width).astype(jnp.bfloat16)
    reading = lax.all_gather(own_read, "tp", axis=0, tiled=True)
    return (key_cache, value_cache, reading)


def solution(mesh):
    placed = (P("sp", None), P(), P(), P(None, "tp"), P(None, "tp"), P(None, "tp"), P("sp", "tp"))
    return jax.shard_map(
        shards,
        mesh=mesh,
        in_specs=placed,
        out_specs=(P("sp", None, None, "tp"), P("sp", None, None, "tp"), P()),
        check_vma=False,
    )
```

profile of v0, /device:TPU:0, one launch (start us, length us, event | category | flops | bytes accessed | tf_op | source)
XLA Modules:
  0.0 65.4 jit_solution(9334492287471043287)
XLA Ops:
  0.6 0.0 copy-start
  0.7 1.7 %fusion = f32[288]{0:T(512)S(1)} fusion(bf16[288,2048]{1,0:T(8,128)(2,1)} %param.7), kind=kLoop, calls=%fused_computation.2 | loop fusion | flops 1769184 | bytes 1180800 | tf_op jit(solution)/shard_map/reduce_sum | solution.py:11
  2.4 0.2 copy-done.1
  2.6 1.3 %convolution_convert_fusion = bf16[288,256]{1,0:T(8,128)(2,1)S(1)} fusion(bf16[2048,256]{1,0:T(8,128)(2,1)S(1)} %copy-done, bf16[288,2048]{1,0:T(8,128)(2,1)S(1)} %copy-done.1, f32[2048]{0:T(1024)} %param.9, f32[288]{0:T(512)S(1)} %add_rsqrt_fusion), kind=kOutput, calls=%fused_computation.5 | convolution fusion | flops 304422912 | bytes 2385024 | tf_op jit(solution)/shard_map/dot_general | solution.py:24
  3.9 0.5 convolution_convert_fusion.1
  4.5 0.0 copy-start.3
  4.5 0.0 copy-start.2
  4.6 0.0 copy-start.7
  4.6 0.0 copy-start.4
  4.6 1.0 %copy.17 = bf16[2,8,1,36,256]{4,0,3,2,1:T(2,128)(2,1)} copy(bf16[2,8,1,36,256]{4,3,1,2,0:T(8,128)(2,1)S(1)} %pad_maximum_fusion) | data formatting | bytes 589824 | tf_op jit(solution)/shard_map/stack | solution.py:25
  5.6 7.3 %all-to-all-start = ((bf16[2,8,1,36,256]{4,0,3,2,1:T(2,128)(2,1)}), bf16[2,8,1,36,256]{4,0,3,2,1:T(2,128)(2,1)S(1)}, u32[]{:S(2)}, u32[]{:S(2)}) async-start(bf16[2,8,1,36,256]{4,0,3,2,1:T(2,128)(2,1)} %copy.17), calls=%async_computation | async-start | bytes 589824 | tf_op jit(solution)/shard_map/all_to_all | solution.py:26
  13.0 0.6 fusion.11
  14.3 0.2 fusion.21
  14.5 0.1 fusion.8
  14.7 0.6 dynamic-slice
  16.0 0.1 fusion.19
  16.1 0.1 negate_dynamic-update-slice_fusion
  16.2 21.8 %all-reduce.1 = f32[16]{0:T(128)S(1)} all-reduce(f32[16]{0:T(128)S(1)} %negate_dynamic-update-slice_fusion), channel_id=2, replica_groups=mesh['sp'=8,'tp'=4] {'sp'}, use_global_device_ids=true, to_apply=%add.1 | all-reduce | flops 16 | bytes 128
  38.1 2.5 %reduce-window.6 = f32[2,3,128]{2,1,0:T(4,128)S(1)} reduce-window(f32[2,3,128]{2,1,0:T(4,128)S(1)} %reshape.81, f32[]{:T(128)} %constant.20.clone.1), window={size=1x1x128 pad=0_0x0_0x0_127}, to_apply=%region_2.3 | reduce-window | flops 97536 | bytes 6148 | tf_op jit(solution)/shard_map/reduce-window
  40.6 0.1 slice_reduce_fusion
  40.7 0.2 reduce-window.9
  40.9 0.1 slice.21
  40.9 0.1 add_bitcast_fusion
  41.0 0.1 reshape.84
  41.1 0.1 select_reduce_fusion
  41.2 0.1 exponential_bitcast_fusion
  41.3 0.1 fusion.5
  41.4 17.1 %psum.7 = bf16[2,128]{1,0:T(2,128)(2,1)S(1)} all-reduce(f32[2,128]{1,0:T(2,128)S(1)} %bitcast.64), channel_id=1, replica_groups=mesh['sp'=8,'tp'=4] {'sp'}, use_global_device_ids=true, to_apply=%region_6.7 | all-reduce | flops 256 | bytes 1536 | tf_op jit(solution)/shard_map/psum | solution.py:48
  58.6 5.1 %all-gather.1 = bf16[4,1,256]{2,1,0:T(2,128)(2,1)S(1)} all-gather(bf16[1,1,256]{2,1,0:T(2,128)(2,1)S(1)} %reshape.88), channel_id=1, replica_groups=mesh['sp'=8,'tp'=4] {'tp'}, dimensions={0}, use_global_device_ids=true | all-gather | bytes 2560 | tf_op jit(solution)/shard_map/all_gather | solution.py:50
  63.6 0.6 copy.31
  64.2 0.4 fusion.20
  64.6 0.8 %copy_bitcast_fusion = (bf16[1,8,36,256]{3,1,2,0:T(8,128)(2,1)}, bf16[1,8,36,256]{3,1,2,0:T(8,128)(2,1)}) fusion(bf16[1,8,1,36,256]{4,0,3,2,1:T(2,128)(2,1)S(1)} %get-tuple-element.11, bf16[1,8,1,36,256]{4,0,3,2,1:T(2,128)(2,1)S(1)} %get-tuple-element.12), kind=kLoop, calls=%fused_computation.14 | loop fusion | bytes 589824 | tf_op jit(solution)/shard_map/squeeze | solution.py:28
  (26 shorter events, 0.2 us)
Async XLA Ops:
  0.6 1.8 %copy-start = (bf16[2048,256]{1,0:T(8,128)(2,1)S(1)}, bf16[2048,256]{1,0:T(8,128)(2,1)}, u32[]{:S(2)}) copy-start(bf16[2048,256]{1,0:T(8,128)(2,1)} %param.11) | copy-start | bytes 3145732
  0.6 1.9 %copy-start.1 = (bf16[288,2048]{1,0:T(8,128)(2,1)S(1)}, bf16[288,2048]{1,0:T(8,128)(2,1)}, u32[]{:S(2)}) copy-start(bf16[288,2048]{1,0:T(8,128)(2,1)} %param.7) | copy-start | bytes 3538948
  2.6 1.3 %copy-start.5 = (f32[2048]{0:T(1024)S(1)}, f32[2048]{0:T(1024)}, u32[]{:S(2)}) copy-start(f32[2048]{0:T(1024)} %param.9) | copy-start | bytes 24580
  2.6 1.3 %copy-start.6 = (bf16[2048,256]{1,0:T(8,128)(2,1)S(1)}, bf16[2048,256]{1,0:T(8,128)(2,1)}, u32[]{:S(2)}) copy-start(bf16[2048,256]{1,0:T(8,128)(2,1)} %param.10) | copy-start | bytes 3145732
  4.5 8.5 %copy-start.3 = (bf16[2048]{0:T(1024)(128)(2,1)S(1)}, bf16[2048]{0:T(1024)(128)(2,1)}, u32[]{:S(2)}) copy-start(bf16[2048]{0:T(1024)(128)(2,1)} %param.8) | copy-start | bytes 12292
  4.5 9.8 %copy-start.2 = (bf16[2048,256]{1,0:T(8,128)(2,1)S(1)}, bf16[2048,256]{1,0:T(8,128)(2,1)}, u32[]{:S(2)}) copy-start(bf16[2048,256]{1,0:T(8,128)(2,1)} %param.12) | copy-start | bytes 3145732
  4.6 10.1 %copy-start.7 = (u32[32]{0:T(128)S(1)}, u32[32]{0:T(128)}, u32[]{:S(2)}) copy-start(u32[32]{0:T(128)} %constant.31) | copy-start | bytes 388
  4.6 11.3 %copy-start.4 = (f32[288,2]{0,1:T(2,128)S(1)}, f32[288,2]{0,1:T(2,128)}, u32[]{:S(2)}) copy-start(f32[288,2]{0,1:T(2,128)} %param.13) | copy-start | bytes 6916
  5.6 58.6 %all-to-all-start = ((bf16[2,8,1,36,256]{4,0,3,2,1:T(2,128)(2,1)}), bf16[2,8,1,36,256]{4,0,3,2,1:T(2,128)(2,1)S(1)}, u32[]{:S(2)}, u32[]{:S(2)}) async-start(bf16[2,8,1,36,256]{4,0,3,2,1:T(2,128)(2,1)} %copy.17), calls=%async_computation | async-start | bytes 589824 | tf_op jit(solution)/shard_map/all_to_all | solution.py:26
where the time goes:
time: 65.7 us; the launch traced here: 65.4 us
  blocking collectives  44 us (67%)
  starting transfers between devices  7.31 us (11%)
  other arithmetic  5.61 us (9%)
  local copies, waits for them, and re-layouts  3.98 us (6%)
  matrix products  2.36 us (4%)
  between operations  2.15 us (3%)
    unnamed x1, blocking collectives  21.8 us
    psum x1, blocking collectives, shards(): summed = lax.psum(partial_value, 'sp')  17.1 us
    all_to_all x1, starting transfers between devices, shards(): lax.all_to_all(outgoing, 'sp', split_axis=1, concat_axis=2, tiled=True)  7.31 us
    all_gather x1, blocking collectives, shards(): reading = lax.all_gather(own_read, 'tp', axis=0, tiled=True)  5.05 us
    another operation x2, other arithmetic  2.71 us
    reduce_sum x2, other arithmetic, norm_rows(): jnp.mean(wide_rows * wide_rows, axis=-1, keepdims=True) + 1e-06  2.34 us
    unnamed x21, local copies, waits for them, and re-layouts  1.43 us
  transfers between devices with their start and end apart: 1, of which 0 were waited for; matrix products, arithmetic and copies ran while one was open for 9% of the time, Pallas kernels for 0%

commit v1 on v0

v1 whole, which is shorter than its diff:
```python
import functools

import jax
import jax.numpy as jnp
from jax import lax
from jax.experimental import pallas as pl
from jax.experimental.pallas import tpu as pltpu
from jax.sharding import PartitionSpec as P

HEAD_DIM = 128
MESH = pl.DeviceIdType.MESH


def norm_rows(rows, gain):
    wide = rows.astype(jnp.float32)
    inv_rms = lax.rsqrt(jnp.mean(wide * wide, axis=-1, keepdims=True) + 1e-06)
    return (wide * inv_rms * gain).astype(jnp.bfloat16)


def split_parts(wide, count):
    parts = []
    for _ in range(count):
        part = wide.astype(jnp.bfloat16).astype(jnp.float32)
        parts.append(part)
        wide = wide - part
    return jnp.concatenate(parts, axis=0).astype(jnp.bfloat16)


def fold_parts(rows, heads):
    total = rows[:heads]
    for first in range(heads, rows.shape[0], heads):
        total = total + rows[first : first + heads]
    return total


def kernel(
    n_sp, n_tp, chunks,
    x_hbm, next_hbm, gain_hbm, wk_hbm, wv_hbm, wq_hbm, offset_hbm,
    k_out, v_out, read_out,
    x_in, normed, next_in, gain_in, wk, wv, wq, offset,
    k_send, v_send, message, gathered, head_message, head_gathered,
    x_sem, load_sem, own_sem,
    k_ssem, k_rsem, v_ssem, v_rsem, m_ssem, m_rsem, h_ssem, h_rsem,
):
    me = lax.axis_index("sp")
    lane = lax.axis_index("tp")
    span, width = x_hbm.shape[0], wk_hbm.shape[1]
    heads = width // HEAD_DIM
    sub = span // n_sp
    rows = span // chunks

    loads = [
        pltpu.make_async_copy(hbm, vmem, load_sem.at[n])
        for n, (hbm, vmem) in enumerate(
            [
                (gain_hbm, gain_in),
                (wk_hbm, wk),
                (wv_hbm, wv),
                (next_hbm, next_in),
                (wq_hbm, wq),
                (offset_hbm, offset),
            ]
        )
    ]
    x_loads = [
        pltpu.make_async_copy(
            x_hbm.at[pl.ds(c * rows, rows)], x_in.at[pl.ds(c * rows, rows)], x_sem.at[c]
        )
        for c in range(chunks)
    ]
    loads[0].start()
    for load in x_loads:
        load.start()
    for load in loads[1:]:
        load.start()

    barrier = pltpu.get_barrier_semaphore()

    @pl.loop(1, n_sp)
    def _(step):
        pl.semaphore_signal(
            barrier, inc=1, device_id=(lax.rem(me + step, n_sp), lane), device_id_type=MESH
        )

    @pl.loop(1, n_tp)
    def _(step):
        pl.semaphore_signal(
            barrier, inc=1, device_id=(me, lax.rem(lane + step, n_tp)), device_id_type=MESH
        )

    loads[0].wait()
    gain = gain_in[...]
    step_rows = 16 if rows % 16 == 0 else rows
    for c in range(chunks):
        x_loads[c].wait()
        for first in range(c * rows, (c + 1) * rows, step_rows):
            normed[first : first + step_rows, :] = norm_rows(x_in[first : first + step_rows, :], gain)

    def copies(step, send, recv, ssem, rsem):
        to = lax.rem(me + step, n_sp)
        return pltpu.make_async_remote_copy(
            src_ref=send.at[to], dst_ref=recv.at[me],
            send_sem=ssem.at[step], recv_sem=rsem.at[step],
            device_id=(to, lane), device_id_type=MESH,
        )

    def project(weight, send):
        wide = jnp.dot(normed[...], weight[...], preferred_element_type=jnp.float32)
        for slot in range(n_sp):
            send[slot] = wide[slot * sub : (slot + 1) * sub].astype(jnp.bfloat16)
        return wide.astype(jnp.bfloat16)

    loads[1].wait()
    keys = project(wk, k_send)
    pl.semaphore_wait(barrier, n_sp + n_tp - 2)

    @pl.loop(1, n_sp)
    def _(step):
        copies(step, k_send, k_out, k_ssem, k_rsem).start()

    own_key = pltpu.make_async_copy(k_send.at[me], k_out.at[me], own_sem.at[0])
    own_key.start()

    loads[3].wait()
    loads[4].wait()
    loads[5].wait()
    query_normed = jnp.broadcast_to(norm_rows(next_in[...], gain), (16, x_hbm.shape[1]))
    query = jnp.dot(query_normed, wq[...], preferred_element_type=jnp.float32)
    row_ids = lax.broadcasted_iota(jnp.int32, query.shape, 0)
    head_ids = lax.broadcasted_iota(jnp.int32, query.shape, 1) // HEAD_DIM
    query = jnp.where(row_ids == head_ids, query, 0.0).astype(jnp.bfloat16)
    logits = lax.dot_general(
        query, keys, (((1,), (1,)), ((), ())), preferred_element_type=jnp.float32
    )[:heads]
    logits = logits * HEAD_DIM ** (-0.5) + offset[...]
    tail = jnp.log1p(jnp.exp(-jnp.abs(logits)))
    log_breaks = -jnp.maximum(logits, 0.0) - tail
    later_than = (
        lax.broadcasted_iota(jnp.int32, (span, span), 0)
        > lax.broadcasted_iota(jnp.int32, (span, span), 1)
    )
    later_than = jnp.where(later_than, 1.0, 0.0).astype(jnp.bfloat16)
    inner = fold_parts(
        jnp.dot(split_parts(log_breaks, 3), later_than, preferred_element_type=jnp.float32), heads
    )
    block_total = jnp.sum(log_breaks, axis=1, keepdims=True)
    weights = jnp.exp(jnp.minimum(logits, 0.0) - tail + inner)

    loads[2].wait()
    values = project(wv, v_send)
    read = fold_parts(
        jnp.dot(split_parts(weights, 2), values, preferred_element_type=jnp.float32), heads
    )
    for head in range(heads):
        message[head : head + 1, :] = read[head : head + 1, head * HEAD_DIM : (head + 1) * HEAD_DIM]
        message[heads + head : heads + head + 1, :] = jnp.broadcast_to(
            block_total[head : head + 1], (1, HEAD_DIM)
        )

    def message_copy(step):
        return pltpu.make_async_remote_copy(
            src_ref=message, dst_ref=gathered.at[me],
            send_sem=m_ssem.at[step], recv_sem=m_rsem.at[step],
            device_id=(lax.rem(me + step, n_sp), lane), device_id_type=MESH,
        )

    @pl.loop(1, n_sp)
    def _(step):
        message_copy(step).start()

    own_message = pltpu.make_async_copy(message, gathered.at[me], own_sem.at[2])
    own_message.start()

    @pl.loop(1, n_sp)
    def _(step):
        copies(step, v_send, v_out, v_ssem, v_rsem).start()

    own_value = pltpu.make_async_copy(v_send.at[me], v_out.at[me], own_sem.at[1])
    own_value.start()

    own_message.wait()

    @pl.loop(1, n_sp)
    def _(step):
        message_copy(step).wait_recv()

    def add_block(step, carry):
        total, carried = carry
        block = gathered[n_sp - 1 - step]
        total = total + jnp.exp(carried) * block[:heads]
        return total, carried + block[heads : 2 * heads]

    zero = jnp.zeros((heads, HEAD_DIM), jnp.float32)
    total, _ = lax.fori_loop(0, n_sp, add_block, (zero, zero), unroll=n_sp <= 16)
    head_message[:heads, :] = total

    def head_copy(step):
        return pltpu.make_async_remote_copy(
            src_ref=head_message, dst_ref=head_gathered.at[lane],
            send_sem=h_ssem.at[step], recv_sem=h_rsem.at[step],
            device_id=(me, lax.rem(lane + step, n_tp)), device_id_type=MESH,
        )

    @pl.loop(1, n_tp)
    def _(step):
        head_copy(step).start()

    own_head = pltpu.make_async_copy(head_message, head_gathered.at[lane], own_sem.at[3])
    own_head.start()
    own_head.wait()

    @pl.loop(1, n_tp)
    def _(step):
        head_copy(step).wait_recv()

    read_out[...] = jnp.concatenate(
        [head_gathered[part, :heads, :] for part in range(n_tp)], axis=0
    ).astype(jnp.bfloat16)

    own_key.wait()
    own_value.wait()

    @pl.loop(1, n_tp)
    def _(step):
        head_copy(step).wait_send()

    @pl.loop(1, n_sp)
    def _(step):
        message_copy(step).wait_send()
        copies(step, k_send, k_out, k_ssem, k_rsem).wait()
        copies(step, v_send, v_out, v_ssem, v_rsem).wait()


def shards(prompt_input, next_input, norm_gain, w_key, w_value, w_query, key_offset):
    span, depth = prompt_input.shape
    width = w_key.shape[1]
    heads = width // HEAD_DIM
    n_sp, n_tp = lax.axis_size("sp"), lax.axis_size("tp")
    sub = span // n_sp
    chunks = 3 if span % 48 == 0 else 1
    message_rows = -(-2 * heads // 8) * 8
    head_rows = -(-heads // 8) * 8
    wide, narrow = jnp.float32, jnp.bfloat16
    cache = jax.ShapeDtypeStruct((n_sp, sub, width), narrow)
    sems = pltpu.SemaphoreType.DMA
    key_cache, value_cache, reading = pl.pallas_call(
        functools.partial(kernel, n_sp, n_tp, chunks),
        out_shape=(cache, cache, jax.ShapeDtypeStruct((n_tp * heads, HEAD_DIM), narrow)),
        in_specs=[pl.BlockSpec(memory_space=pl.ANY)] * 7,
        out_specs=(pl.BlockSpec(memory_space=pltpu.VMEM),) * 3,
        scratch_shapes=[
            pltpu.VMEM((span, depth), narrow),
            pltpu.VMEM((span, depth), narrow),
            pltpu.VMEM((1, depth), wide),
            pltpu.VMEM((1, depth), wide),
            pltpu.VMEM((depth, width), narrow),
            pltpu.VMEM((depth, width), narrow),
            pltpu.VMEM((depth, width), narrow),
            pltpu.VMEM((heads, span), wide),
            pltpu.VMEM((n_sp, sub, width), narrow),
            pltpu.VMEM((n_sp, sub, width), narrow),
            pltpu.VMEM((message_rows, HEAD_DIM), wide),
            pltpu.VMEM((n_sp, message_rows, HEAD_DIM), wide),
            pltpu.VMEM((head_rows, HEAD_DIM), wide),
            pltpu.VMEM((n_tp, head_rows, HEAD_DIM), wide),
            sems((chunks,)),
            sems((6,)),
            sems((4,)),
            sems((n_sp,)),
            sems((n_sp,)),
            sems((n_sp,)),
            sems((n_sp,)),
            sems((n_sp,)),
            sems((n_sp,)),
            sems((n_tp,)),
            sems((n_tp,)),
        ],
        compiler_params=pltpu.CompilerParams(collective_id=0, has_side_effects=True),
        name="prefill",
    )(
        prompt_input,
        next_input.astype(wide)[None],
        norm_gain[None],
        w_key,
        w_value,
        w_query,
        key_offset.T,
    )
    return key_cache[None], value_cache[None], reading.reshape(-1)


def solution(mesh):
    placed = (P("sp", None), P(), P(), P(None, "tp"), P(None, "tp"), P(None, "tp"), P("sp", "tp"))
    return jax.shard_map(
        shards,
        mesh=mesh,
        in_specs=placed,
        out_specs=(P("sp", None, None, "tp"), P("sp", None, None, "tp"), P()),
        check_vma=False,
    )
```

time: 65.7 us -> 26.5 us (0.40)
  blocking collectives: 44 us -> 0 us
  Pallas kernels: 0 us -> 19.8 us
  starting transfers between devices: 7.31 us -> 0 us
  other arithmetic: 5.61 us -> 1.29 us
  matrix products: 2.36 us -> 0 us
  between operations: 2.15 us -> 0.64 us
    unnamed x1 -> x0, blocking collectives: 21.8 us -> none
    pallas_call x0 -> x1, Pallas kernels: none -> 19.8 us  [shards(): pl.pallas_call(functools.partial(kernel, n_sp, n_tp, chunks), out_shape=(...]
    psum x1 -> x0, blocking collectives: 17.1 us -> none  [shards(): summed = lax.psum(partial_value, 'sp')]
    all_to_all x1 -> x0, starting transfers between devices: 7.31 us -> none  [shards(): lax.all_to_all(outgoing, 'sp', split_axis=1, concat_axis=2, tiled=True)]
    all_gather x1 -> x0, blocking collectives: 5.05 us -> none  [shards(): reading = lax.all_gather(own_read, 'tp', axis=0, tiled=True)]
    unnamed x21 -> x3, local copies, waits for them, and re-layouts: 1.43 us -> 4.46 us
    another operation x3 -> x0, other arithmetic: 2.74 us -> none
    reduce_sum x4 -> x0, other arithmetic: 2.56 us -> none  [the longest x2 2.34 us: norm_rows(): jnp.mean(wide_rows * wide_rows, axis=-1, keepdims=True) + 1e-06]
  transfers between devices with their start and end apart: 1 -> 0, of which waited for: 0 -> 0; matrix products, arithmetic and copies ran while one was open for 9% -> 0% of each run, Pallas kernels for 0% -> 0%
where the time goes in v1:
time: 26.5 us; the launch traced here: 26.2 us
  Pallas kernels  19.8 us (75%)
  local copies, waits for them, and re-layouts  4.46 us (17%)
  other arithmetic  1.29 us (5%)
  between operations  0.64 us (2%)
    pallas_call x1, Pallas kernels, shards(): pl.pallas_call(functools.partial(kernel, n_sp, n_tp, chunks), out_shape=(...  19.8 us
    unnamed x3, local copies, waits for them, and re-layouts  4.46 us
    broadcast_in_dim x1, other arithmetic, shards(): next_input.astype(wide)[None]  1.29 us

profile of v1, /device:TPU:0, one launch (start us, length us, event | category | flops | bytes accessed | tf_op | source)
XLA Modules:
  0.0 26.2 jit_solution(16098770422184567267)
XLA Ops:
  0.6 1.3 %broadcast_in_dim.19 = f32[2048]{0:T(1024)} convert(bf16[2048]{0:T(1024)(128)(2,1)} %param.8) | non-fusion elementwise | flops 2048 | bytes 12288 | tf_op jit(solution)/shard_map/broadcast_in_dim | solution.py:282
  1.9 19.8 %prefill.1 = (bf16[8,36,256]{2,1,0:T(8,128)(2,1)}, bf16[8,36,256]{2,1,0:T(8,128)(2,1)}, bf16[8,128]{1,0:T(8,128)(2,1)}) custom-call(bf16[288,2048]{1,0:T(8,128)(2,1)} %x_hbm.1, f32[1,2048]{1,0:T(1,128)} %bitcast.8, f32[1,2048]{1,0:T(1,128)} %bitcast.9, bf16[2048,256]{1,0:T(8,128)(2,1)} %wk_hbm.1, bf16[2048,256]{1,0:T(8,128)(2,1)} %wv_hbm.1, ...), custom_call_target="tpu_custom_call" | custom-call | tf_op jit(solution)/shard_map/prefill/pallas_call | solution.py:246
  21.7 1.6 %copy.10 = bf16[1,8,36,256]{3,1,2,0:T(8,128)(2,1)} copy(bf16[1,8,36,256]{3,2,1,0:T(8,128)(2,1)} %bitcast.7) | data formatting | bytes 294912
  23.3 1.6 %copy.11 = bf16[1,8,36,256]{3,1,2,0:T(8,128)(2,1)} copy(bf16[1,8,36,256]{3,2,1,0:T(8,128)(2,1)} %bitcast.6) | data formatting | bytes 294912
  24.9 1.3 %copy.13 = bf16[1024]{0:T(1024)(128)(2,1)} copy(bf16[1024]{0:T(1024)(128)(2,1)} %bitcast.11) | data formatting | bytes 4096

commit v2 on v1

--- a/solution.py
+++ b/solution.py
@@ -124,7 +124,9 @@
     loads[3].wait()
     loads[4].wait()
     loads[5].wait()
-    query_normed = jnp.broadcast_to(norm_rows(next_in[...], gain), (16, x_hbm.shape[1]))
+    next_row = next_in[...].astype(jnp.float32)
+    next_row = jnp.concatenate([next_row[n : n + 1] for n in range(next_row.shape[0])], axis=1)
+    query_normed = jnp.broadcast_to(norm_rows(next_row, gain), (16, x_hbm.shape[1]))
     query = jnp.dot(query_normed, wq[...], preferred_element_type=jnp.float32)
     row_ids = lax.broadcasted_iota(jnp.int32, query.shape, 0)
     head_ids = lax.broadcasted_iota(jnp.int32, query.shape, 1) // HEAD_DIM
@@ -231,6 +233,12 @@
         copies(step, v_send, v_out, v_ssem, v_rsem).wait()
 
 
+def finish(k_in, v_in, read_in, k_out, v_out, read_out):
+    for landed, out in ((k_in, k_out), (v_in, v_out)):
+        out[...] = jnp.swapaxes(landed[...].astype(jnp.float32), 0, 1).astype(jnp.bfloat16)
+    read_out[...] = read_in[...]
+
+
 def shards(prompt_input, next_input, norm_gain, w_key, w_value, w_query, key_offset):
     span, depth = prompt_input.shape
     width = w_key.shape[1]
@@ -243,15 +251,15 @@
     wide, narrow = jnp.float32, jnp.bfloat16
     cache = jax.ShapeDtypeStruct((n_sp, sub, width), narrow)
     sems = pltpu.SemaphoreType.DMA
-    key_cache, value_cache, reading = pl.pallas_call(
+    landed = pl.pallas_call(
         functools.partial(kernel, n_sp, n_tp, chunks),
         out_shape=(cache, cache, jax.ShapeDtypeStruct((n_tp * heads, HEAD_DIM), narrow)),
-        in_specs=[pl.BlockSpec(memory_space=pl.ANY)] * 7,
+        in_specs=[pl.BlockSpec(memory_space=pltpu.HBM)] * 7,
         out_specs=(pl.BlockSpec(memory_space=pltpu.VMEM),) * 3,
         scratch_shapes=[
             pltpu.VMEM((span, depth), narrow),
             pltpu.VMEM((span, depth), narrow),
-            pltpu.VMEM((1, depth), wide),
+            pltpu.VMEM((depth // HEAD_DIM, HEAD_DIM), narrow),
             pltpu.VMEM((1, depth), wide),
             pltpu.VMEM((depth, width), narrow),
             pltpu.VMEM((depth, width), narrow),
@@ -275,18 +283,38 @@
             sems((n_tp,)),
             sems((n_tp,)),
         ],
-        compiler_params=pltpu.CompilerParams(collective_id=0, has_side_effects=True),
+        compiler_params=pltpu.CompilerParams(
+            collective_id=0, has_side_effects=True, vmem_limit_bytes=16 * 2**20
+        ),
         name="prefill",
     )(
-        prompt_input,
-        next_input.astype(wide)[None],
-        norm_gain[None],
-        w_key,
-        w_value,
-        w_query,
-        key_offset.T,
-    )
-    return key_cache[None], value_cache[None], reading.reshape(-1)
+        *[
+            pltpu.with_memory_space_constraint(operand, pltpu.HBM)
+            for operand in (
+                prompt_input,
+                next_input.reshape(-1, HEAD_DIM),
+                norm_gain[None],
+                w_key,
+                w_value,
+                w_query,
+                key_offset.T,
+            )
+        ]
+    )
+    slotted = jax.ShapeDtypeStruct((sub, n_sp, width), narrow)
+    key_cache, value_cache, reading = pl.pallas_call(
+        finish,
+        out_shape=(slotted, slotted, jax.ShapeDtypeStruct((n_tp * heads, HEAD_DIM), narrow)),
+        in_specs=[pl.BlockSpec(memory_space=pltpu.VMEM)] * 3,
+        out_specs=(pl.BlockSpec(memory_space=pltpu.VMEM),) * 3,
+        compiler_params=pltpu.CompilerParams(vmem_limit_bytes=16 * 2**20),
+        name="finish",
+    )(*landed)
+    return (
+        jnp.swapaxes(key_cache, 0, 1)[None],
+        jnp.swapaxes(value_cache, 0, 1)[None],
+        reading.reshape(-1),
+    )
 
 
 def solution(mesh):

time: 26.5 us -> 20.8 us (0.78)
  local copies, waits for them, and re-layouts: 4.46 us -> 0 us
  other arithmetic: 1.29 us -> 0 us
    unnamed x3 -> x0, local copies, waits for them, and re-layouts: 4.46 us -> none
    broadcast_in_dim x1 -> x0, other arithmetic: 1.29 us -> none  [shards(): next_input.astype(wide)[None]]
    pallas_call x0 -> x1, Pallas kernels: none -> 0.8 us  [shards(): pl.pallas_call(finish, out_shape=(slotted, slotted, jax.ShapeDtypeStruct(...]
    pallas_call x1, Pallas kernels: 19.8 us -> 19.1 us  [shards(): pl.pallas_call(functools.partial(kernel, n_sp, n_tp, chunks), out_shape=(...]
where the time goes in v2:
time: 20.8 us; the launch traced here: 20.5 us
  Pallas kernels  19.9 us (96%)
  between operations  0.64 us (3%)
    pallas_call x1, Pallas kernels, shards(): pl.pallas_call(functools.partial(kernel, n_sp, n_tp, chunks), out_shape=(...  19.1 us
    pallas_call x1, Pallas kernels, shards(): pl.pallas_call(finish, out_shape=(slotted, slotted, jax.ShapeDtypeStruct(...  0.8 us

profile of v2, /device:TPU:0, one launch (start us, length us, event | category | flops | bytes accessed | tf_op | source)
XLA Modules:
  0.0 20.5 jit_solution(8941375964076374138)
XLA Ops:
  0.6 19.1 %prefill.1 = (bf16[8,36,256]{2,1,0:T(8,128)(2,1)S(1)}, bf16[8,36,256]{2,1,0:T(8,128)(2,1)S(1)}, bf16[8,128]{1,0:T(8,128)(2,1)S(1)}) custom-call(bf16[288,2048]{1,0:T(8,128)(2,1)} %x_hbm.1, bf16[16,128]{1,0:T(8,128)(2,1)} %bitcast.11, f32[1,2048]{1,0:T(1,128)} %bitcast.10, bf16[2048,256]{1,0:T(8,128)(2,1)} %wk_hbm.1, bf16[2048,256]{1,0:T(8,128)(2,1)} %wv_hbm.1, ...), custom_call_target="tpu_custom_call" | custom-call | tf_op jit(solution)/shard_map/prefill/pallas_call | solution.py:254
  19.7 0.8 %finish.1 = (bf16[36,8,256]{2,1,0:T(8,128)(2,1)}, bf16[36,8,256]{2,1,0:T(8,128)(2,1)}, bf16[8,128]{1,0:T(8,128)(2,1)}) custom-call(bf16[8,36,256]{2,1,0:T(8,128)(2,1)S(1)} %get-tuple-element.9.k_in, bf16[8,36,256]{2,1,0:T(8,128)(2,1)S(1)} %get-tuple-element.10.v_in, bf16[8,128]{1,0:T(8,128)(2,1)S(1)} %get-tuple-element.11.read_in), custom_call_target="tpu_custom_call" | custom-call | tf_op jit(solution)/shard_map/finish/pallas_call | solution.py:305

commit v3 on v2

--- a/solution.py
+++ b/solution.py
@@ -36,11 +36,11 @@
 def kernel(
     n_sp, n_tp, chunks,
     x_hbm, next_hbm, gain_hbm, wk_hbm, wv_hbm, wq_hbm, offset_hbm,
-    k_out, v_out, read_out,
+    landed, read_out,
     x_in, normed, next_in, gain_in, wk, wv, wq, offset,
-    k_send, v_send, message, gathered, head_message, head_gathered,
+    outgoing, message, gathered, head_message, head_gathered,
     x_sem, load_sem, own_sem,
-    k_ssem, k_rsem, v_ssem, v_rsem, m_ssem, m_rsem, h_ssem, h_rsem,
+    b_ssem, b_rsem, m_ssem, m_rsem, h_ssem, h_rsem,
 ):
     me = lax.axis_index("sp")
     lane = lax.axis_index("tp")
@@ -49,16 +49,16 @@
     sub = span // n_sp
     rows = span // chunks
 
-    loads = [
+    load_gain, load_next, load_offset, load_key, load_query, load_value = [
         pltpu.make_async_copy(hbm, vmem, load_sem.at[n])
         for n, (hbm, vmem) in enumerate(
             [
                 (gain_hbm, gain_in),
+                (next_hbm, next_in),
+                (offset_hbm, offset),
                 (wk_hbm, wk),
+                (wq_hbm, wq),
                 (wv_hbm, wv),
-                (next_hbm, next_in),
-                (wq_hbm, wq),
-                (offset_hbm, offset),
             ]
         )
     ]
@@ -68,11 +68,12 @@
         )
         for c in range(chunks)
     ]
-    loads[0].start()
+    load_gain.start()
     for load in x_loads:
         load.start()
-    for load in loads[1:]:
-        load.start()
+    load_key.start()
+    load_next.start()
+    load_offset.start()
 
     barrier = pltpu.get_barrier_semaphore()
 
@@ -88,42 +89,25 @@
             barrier, inc=1, device_id=(me, lax.rem(lane + step, n_tp)), device_id_type=MESH
         )
 
-    loads[0].wait()
+    load_gain.wait()
     gain = gain_in[...]
     step_rows = 16 if rows % 16 == 0 else rows
     for c in range(chunks):
         x_loads[c].wait()
+        if c == 0:
+            load_query.start()
+        if c == chunks - 1:
+            load_value.start()
         for first in range(c * rows, (c + 1) * rows, step_rows):
             normed[first : first + step_rows, :] = norm_rows(x_in[first : first + step_rows, :], gain)
 
-    def copies(step, send, recv, ssem, rsem):
-        to = lax.rem(me + step, n_sp)
-        return pltpu.make_async_remote_copy(
-            src_ref=send.at[to], dst_ref=recv.at[me],
-            send_sem=ssem.at[step], recv_sem=rsem.at[step],
-            device_id=(to, lane), device_id_type=MESH,
-        )
-
-    def project(weight, send):
-        wide = jnp.dot(normed[...], weight[...], preferred_element_type=jnp.float32)
-        for slot in range(n_sp):
-            send[slot] = wide[slot * sub : (slot + 1) * sub].astype(jnp.bfloat16)
-        return wide.astype(jnp.bfloat16)
-
-    loads[1].wait()
-    keys = project(wk, k_send)
-    pl.semaphore_wait(barrier, n_sp + n_tp - 2)
-
-    @pl.loop(1, n_sp)
-    def _(step):
-        copies(step, k_send, k_out, k_ssem, k_rsem).start()
-
-    own_key = pltpu.make_async_copy(k_send.at[me], k_out.at[me], own_sem.at[0])
-    own_key.start()
-
-    loads[3].wait()
-    loads[4].wait()
-    loads[5].wait()
+    load_key.wait()
+    wide_keys = jnp.dot(normed[...], wk[...], preferred_element_type=jnp.float32)
+    keys = wide_keys.astype(jnp.bfloat16)
+
+    load_next.wait()
+    load_offset.wait()
+    load_query.wait()
     next_row = next_in[...].astype(jnp.float32)
     next_row = jnp.concatenate([next_row[n : n + 1] for n in range(next_row.shape[0])], axis=1)
     query_normed = jnp.broadcast_to(norm_rows(next_row, gain), (16, x_hbm.shape[1]))
@@ -131,6 +115,8 @@
     row_ids = lax.broadcasted_iota(jnp.int32, query.shape, 0)
     head_ids = lax.broadcasted_iota(jnp.int32, query.shape, 1) // HEAD_DIM
     query = jnp.where(row_ids == head_ids, query, 0.0).astype(jnp.bfloat16)
+
+    load_value.wait()
     logits = lax.dot_general(
         query, keys, (((1,), (1,)), ((), ())), preferred_element_type=jnp.float32
     )[:heads]
@@ -148,16 +134,31 @@
     block_total = jnp.sum(log_breaks, axis=1, keepdims=True)
     weights = jnp.exp(jnp.minimum(logits, 0.0) - tail + inner)
 
-    loads[2].wait()
-    values = project(wv, v_send)
+    wide_values = jnp.dot(normed[...], wv[...], preferred_element_type=jnp.float32)
     read = fold_parts(
-        jnp.dot(split_parts(weights, 2), values, preferred_element_type=jnp.float32), heads
+        jnp.dot(
+            split_parts(weights, 2),
+            wide_values.astype(jnp.bfloat16),
+            preferred_element_type=jnp.float32,
+        ),
+        heads,
     )
     for head in range(heads):
         message[head : head + 1, :] = read[head : head + 1, head * HEAD_DIM : (head + 1) * HEAD_DIM]
         message[heads + head : heads + head + 1, :] = jnp.broadcast_to(
             block_total[head : head + 1], (1, HEAD_DIM)
         )
+    for slot in range(n_sp):
+        outgoing[slot] = jnp.concatenate(
+            [
+                wide[slot * sub : (slot + 1) * sub, head * HEAD_DIM : (head + 1) * HEAD_DIM]
+                for wide in (wide_keys, wide_values)
+                for head in range(heads)
+            ],
+            axis=0,
+        ).astype(jnp.bfloat16)
+
+    pl.semaphore_wait(barrier, n_sp + n_tp - 2)
 
     def message_copy(step):
         return pltpu.make_async_remote_copy(
@@ -166,20 +167,26 @@
             device_id=(lax.rem(me + step, n_sp), lane), device_id_type=MESH,
         )
 
+    def block_copy(step):
+        to = lax.rem(me + step, n_sp)
+        return pltpu.make_async_remote_copy(
+            src_ref=outgoing.at[to], dst_ref=landed.at[me],
+            send_sem=b_ssem.at[step], recv_sem=b_rsem.at[step],
+            device_id=(to, lane), device_id_type=MESH,
+        )
+
     @pl.loop(1, n_sp)
     def _(step):
         message_copy(step).start()
 
-    own_message = pltpu.make_async_copy(message, gathered.at[me], own_sem.at[2])
+    @pl.loop(1, n_sp)
+    def _(step):
+        block_copy(step).start()
+
+    own_message = pltpu.make_async_copy(message, gathered.at[me], own_sem.at[0])
     own_message.start()
-
-    @pl.loop(1, n_sp)
-    def _(step):
-        copies(step, v_send, v_out, v_ssem, v_rsem).start()
-
-    own_value = pltpu.make_async_copy(v_send.at[me], v_out.at[me], own_sem.at[1])
-    own_value.start()
-
+    own_block = pltpu.make_async_copy(outgoing.at[me], landed.at[me], own_sem.at[1])
+    own_block.start()
     own_message.wait()
 
     @pl.loop(1, n_sp)
@@ -194,7 +201,7 @@
 
     zero = jnp.zeros((heads, HEAD_DIM), jnp.float32)
     total, _ = lax.fori_loop(0, n_sp, add_block, (zero, zero), unroll=n_sp <= 16)
-    head_message[:heads, :] = total
+    head_message[...] = total
 
     def head_copy(step):
         return pltpu.make_async_remote_copy(
@@ -207,7 +214,7 @@
     def _(step):
         head_copy(step).start()
 
-    own_head = pltpu.make_async_copy(head_message, head_gathered.at[lane], own_sem.at[3])
+    own_head = pltpu.make_async_copy(head_message, head_gathered.at[lane], own_sem.at[2])
     own_head.start()
     own_head.wait()
 
@@ -216,11 +223,10 @@
         head_copy(step).wait_recv()
 
     read_out[...] = jnp.concatenate(
-        [head_gathered[part, :heads, :] for part in range(n_tp)], axis=0
+        [head_gathered[part] for part in range(n_tp)], axis=0
     ).astype(jnp.bfloat16)
 
-    own_key.wait()
-    own_value.wait()
+    own_block.wait()
 
     @pl.loop(1, n_tp)
     def _(step):
@@ -229,13 +235,19 @@
     @pl.loop(1, n_sp)
     def _(step):
         message_copy(step).wait_send()
-        copies(step, k_send, k_out, k_ssem, k_rsem).wait()
-        copies(step, v_send, v_out, v_ssem, v_rsem).wait()
-
-
-def finish(k_in, v_in, read_in, k_out, v_out, read_out):
-    for landed, out in ((k_in, k_out), (v_in, v_out)):
-        out[...] = jnp.swapaxes(landed[...].astype(jnp.float32), 0, 1).astype(jnp.bfloat16)
+        block_copy(step).wait()
+
+
+def finish(landed, read_in, k_out, v_out, read_out):
+    sub, _, width = k_out.shape
+    heads = width // HEAD_DIM
+    for n, out in enumerate((k_out, v_out)):
+        for head in range(heads):
+            first = (n * heads + head) * sub
+            piece = landed[...].astype(jnp.float32)[:, first : first + sub, :]
+            out[:, :, head * HEAD_DIM : (head + 1) * HEAD_DIM] = jnp.swapaxes(
+                piece, 0, 1
+            ).astype(jnp.bfloat16)
     read_out[...] = read_in[...]
 
 
@@ -246,16 +258,17 @@
     n_sp, n_tp = lax.axis_size("sp"), lax.axis_size("tp")
     sub = span // n_sp
     chunks = 3 if span % 48 == 0 else 1
-    message_rows = -(-2 * heads // 8) * 8
-    head_rows = -(-heads // 8) * 8
     wide, narrow = jnp.float32, jnp.bfloat16
-    cache = jax.ShapeDtypeStruct((n_sp, sub, width), narrow)
+    blocks = (n_sp, 2 * heads * sub, HEAD_DIM)
     sems = pltpu.SemaphoreType.DMA
     landed = pl.pallas_call(
         functools.partial(kernel, n_sp, n_tp, chunks),
-        out_shape=(cache, cache, jax.ShapeDtypeStruct((n_tp * heads, HEAD_DIM), narrow)),
+        out_shape=(
+            jax.ShapeDtypeStruct(blocks, narrow),
+            jax.ShapeDtypeStruct((n_tp * heads, HEAD_DIM), narrow),
+        ),
         in_specs=[pl.BlockSpec(memory_space=pltpu.HBM)] * 7,
-        out_specs=(pl.BlockSpec(memory_space=pltpu.VMEM),) * 3,
+        out_specs=(pl.BlockSpec(memory_space=pltpu.VMEM),) * 2,
         scratch_shapes=[
             pltpu.VMEM((span, depth), narrow),
             pltpu.VMEM((span, depth), narrow),
@@ -265,17 +278,14 @@
             pltpu.VMEM((depth, width), narrow),
             pltpu.VMEM((depth, width), narrow),
             pltpu.VMEM((heads, span), wide),
-            pltpu.VMEM((n_sp, sub, width), narrow),
-            pltpu.VMEM((n_sp, sub, width), narrow),
-            pltpu.VMEM((message_rows, HEAD_DIM), wide),
-            pltpu.VMEM((n_sp, message_rows, HEAD_DIM), wide),
-            pltpu.VMEM((head_rows, HEAD_DIM), wide),
-            pltpu.VMEM((n_tp, head_rows, HEAD_DIM), wide),
+            pltpu.VMEM(blocks, narrow),
+            pltpu.VMEM((2 * heads, HEAD_DIM), wide),
+            pltpu.VMEM((n_sp, 2 * heads, HEAD_DIM), wide),
+            pltpu.VMEM((heads, HEAD_DIM), wide),
+            pltpu.VMEM((n_tp, heads, HEAD_DIM), wide),
             sems((chunks,)),
             sems((6,)),
-            sems((4,)),
-            sems((n_sp,)),
-            sems((n_sp,)),
+            sems((3,)),
             sems((n_sp,)),
             sems((n_sp,)),
             sems((n_sp,)),
@@ -305,7 +315,7 @@
     key_cache, value_cache, reading = pl.pallas_call(
         finish,
         out_shape=(slotted, slotted, jax.ShapeDtypeStruct((n_tp * heads, HEAD_DIM), narrow)),
-        in_specs=[pl.BlockSpec(memory_space=pltpu.VMEM)] * 3,
+        in_specs=[pl.BlockSpec(memory_space=pltpu.VMEM)] * 2,
         out_specs=(pl.BlockSpec(memory_space=pltpu.VMEM),) * 3,
         compiler_params=pltpu.CompilerParams(vmem_limit_bytes=16 * 2**20),
         name="finish",

time: 20.8 us -> 17 us (0.82)
  Pallas kernels: 19.9 us -> 16.1 us
    pallas_call x1, Pallas kernels: 19.1 us -> 15.3 us  [shards(): pl.pallas_call(functools.partial(kernel, n_sp, n_tp, chunks), out_shape=(...]
where the time goes in v3:
time: 17 us; the launch traced here: 16.8 us
  Pallas kernels  16.1 us (95%)
  between operations  0.64 us (4%)
    pallas_call x1, Pallas kernels, shards(): pl.pallas_call(functools.partial(kernel, n_sp, n_tp, chunks), out_shape=(...  15.3 us
    pallas_call x1, Pallas kernels, shards(): pl.pallas_call(finish, out_shape=(slotted, slotted, jax.ShapeDtypeStruct(...  0.83 us

profile of v3, /device:TPU:0, one launch (start us, length us, event | category | flops | bytes accessed | tf_op | source)
XLA Modules:
  0.0 16.8 jit_solution(3786152099118384467)
XLA Ops:
  0.6 15.3 %prefill.1 = (bf16[8,144,128]{2,1,0:T(8,128)(2,1)S(1)}, bf16[8,128]{1,0:T(8,128)(2,1)S(1)}) custom-call(bf16[288,2048]{1,0:T(8,128)(2,1)} %x_hbm.1, bf16[16,128]{1,0:T(8,128)(2,1)} %bitcast.11, f32[1,2048]{1,0:T(1,128)} %bitcast.10, bf16[2048,256]{1,0:T(8,128)(2,1)} %wk_hbm.1, bf16[2048,256]{1,0:T(8,128)(2,1)} %wv_hbm.1, bf16[2048,256]{1,0:T(8,128)(2,1)} %wq_hbm.1, ...), custom_call_target="tpu_custom_call" | custom-call | tf_op jit(solution)/shard_map/prefill/pallas_call | solution.py:264
  15.9 0.8 %finish.1 = (bf16[36,8,256]{2,1,0:T(8,128)(2,1)}, bf16[36,8,256]{2,1,0:T(8,128)(2,1)}, bf16[8,128]{1,0:T(8,128)(2,1)}) custom-call(bf16[8,144,128]{2,1,0:T(8,128)(2,1)S(1)} %get-tuple-element.8.landed, bf16[8,128]{1,0:T(8,128)(2,1)S(1)} %get-tuple-element.9.read_in), custom_call_target="tpu_custom_call" | custom-call | tf_op jit(solution)/shard_map/finish/pallas_call | solution.py:315

commit v4 on v3

--- a/solution.py
+++ b/solution.py
@@ -148,6 +148,29 @@
         message[heads + head : heads + head + 1, :] = jnp.broadcast_to(
             block_total[head : head + 1], (1, HEAD_DIM)
         )
+    pl.semaphore_wait(barrier, n_sp + n_tp - 2)
+
+    upper = me // ((n_sp + 1) // 2)
+
+    def message_copy(step):
+        return pltpu.make_async_remote_copy(
+            src_ref=message, dst_ref=gathered.at[me],
+            send_sem=m_ssem.at[step], recv_sem=m_rsem.at[step],
+            device_id=(lax.rem(me + step, n_sp), lane), device_id_type=MESH,
+        )
+
+    def block_copy(step):
+        to = lax.rem(me + step, n_sp)
+        return pltpu.make_async_remote_copy(
+            src_ref=outgoing.at[to], dst_ref=landed.at[me],
+            send_sem=b_ssem.at[step], recv_sem=b_rsem.at[step],
+            device_id=(to, lane), device_id_type=MESH,
+        )
+
+    @pl.loop(1, n_sp, unroll=n_sp <= 16)
+    def _(near):
+        message_copy(n_sp - near - upper * (n_sp - 2 * near)).start()
+
     for slot in range(n_sp):
         outgoing[slot] = jnp.concatenate(
             [
@@ -158,30 +181,9 @@
             axis=0,
         ).astype(jnp.bfloat16)
 
-    pl.semaphore_wait(barrier, n_sp + n_tp - 2)
-
-    def message_copy(step):
-        return pltpu.make_async_remote_copy(
-            src_ref=message, dst_ref=gathered.at[me],
-            send_sem=m_ssem.at[step], recv_sem=m_rsem.at[step],
-            device_id=(lax.rem(me + step, n_sp), lane), device_id_type=MESH,
-        )
-
-    def block_copy(step):
-        to = lax.rem(me + step, n_sp)
-        return pltpu.make_async_remote_copy(
-            src_ref=outgoing.at[to], dst_ref=landed.at[me],
-            send_sem=b_ssem.at[step], recv_sem=b_rsem.at[step],
-            device_id=(to, lane), device_id_type=MESH,
-        )
-
     @pl.loop(1, n_sp)
-    def _(step):
-        message_copy(step).start()
-
-    @pl.loop(1, n_sp)
-    def _(step):
-        block_copy(step).start()
+    def _(near):
+        block_copy(n_sp - near - upper * (n_sp - 2 * near)).start()
 
     own_message = pltpu.make_async_copy(message, gathered.at[me], own_sem.at[0])
     own_message.start()
@@ -210,7 +212,7 @@
             device_id=(me, lax.rem(lane + step, n_tp)), device_id_type=MESH,
         )
 
-    @pl.loop(1, n_tp)
+    @pl.loop(1, n_tp, unroll=True)
     def _(step):
         head_copy(step).start()
 

time: 17 us -> 17 us (level)
  no operation moved by 1% of the time
where the time goes in v4:
time: 17 us; the launch traced here: 16.7 us
  Pallas kernels  16.1 us (95%)
  between operations  0.64 us (4%)
    pallas_call x1, Pallas kernels, shards(): pl.pallas_call(functools.partial(kernel, n_sp, n_tp, chunks), out_shape=(...  15.3 us
    pallas_call x1, Pallas kernels, shards(): pl.pallas_call(finish, out_shape=(slotted, slotted, jax.ShapeDtypeStruct(...  0.83 us

profile of v4, /device:TPU:0, one launch (start us, length us, event | category | flops | bytes accessed | tf_op | source)
XLA Modules:
  0.0 16.7 jit_solution(15342544415194230661)
XLA Ops:
  0.6 15.3 %prefill.1 = (bf16[8,144,128]{2,1,0:T(8,128)(2,1)S(1)}, bf16[8,128]{1,0:T(8,128)(2,1)S(1)}) custom-call(bf16[288,2048]{1,0:T(8,128)(2,1)} %x_hbm.1, bf16[16,128]{1,0:T(8,128)(2,1)} %bitcast.11, f32[1,2048]{1,0:T(1,128)} %bitcast.10, bf16[2048,256]{1,0:T(8,128)(2,1)} %wk_hbm.1, bf16[2048,256]{1,0:T(8,128)(2,1)} %wv_hbm.1, bf16[2048,256]{1,0:T(8,128)(2,1)} %wq_hbm.1, ...), custom_call_target="tpu_custom_call" | custom-call | tf_op jit(solution)/shard_map/prefill/pallas_call | solution.py:266
  15.9 0.8 %finish.1 = (bf16[36,8,256]{2,1,0:T(8,128)(2,1)}, bf16[36,8,256]{2,1,0:T(8,128)(2,1)}, bf16[8,128]{1,0:T(8,128)(2,1)}) custom-call(bf16[8,144,128]{2,1,0:T(8,128)(2,1)S(1)} %get-tuple-element.8.landed, bf16[8,128]{1,0:T(8,128)(2,1)S(1)} %get-tuple-element.9.read_in), custom_call_target="tpu_custom_call" | custom-call | tf_op jit(solution)/shard_map/finish/pallas_call | solution.py:317
